TPU v7x, 256 devices: a 4x2x16 block of a 4x16x16 slice. The times are simulated.
256 devices in a mesh: grp: 2 (over y), fs: 16 (over z), tp: 8 (over x, core).
Axes of the slice: x: 4, y: 2, z: 16, core: 2. Of those that a mesh axis runs over, the one named last changes fastest.
The devices are a block of a 4x16x16 slice.
Arguments:
- tokens: bfloat16 [16384, 2048], P(('grp', 'fs'), 'tp'), parts along dimension 0, may hold values from -16 to 16
- attn_gain: float32 [2048], replicated, may hold values from 0.1 to 1.9
- w_query: bfloat16 [2048, 1024], P('fs', 'tp'), may hold values from -0.125 to 0.125
- w_key: bfloat16 [2048, 1024], P('fs', 'tp'), may hold values from -0.125 to 0.125
- w_value: bfloat16 [2048, 2048], P('fs', 'tp'), may hold values from -0.125 to 0.125
- w_low: bfloat16 [2048, 32], replicated, may hold values from -0.125 to 0.125
- w_lift: bfloat16 [32, 1024], P(None, 'tp'), may hold values from -1 to 1
- decay_bias: float32 [1024], P('tp'), may hold values from -0.5 to 6
- head_gain: float32 [256], replicated, may hold values from 0.1 to 1.9
- w_out: bfloat16 [2048, 2048], P('tp', 'fs'), may hold values from -0.125 to 0.125
- ffn_gain: float32 [2048], replicated, may hold values from 0.1 to 1.9
- w_gate: bfloat16 [2048, 5632], P('fs', 'tp'), may hold values from -0.125 to 0.125
- w_up: bfloat16 [2048, 5632], P('fs', 'tp'), may hold values from -0.125 to 0.125
- w_down: bfloat16 [5632, 2048], P('tp', 'fs'), may hold values from -0.078125 to 0.078125
- final_gain: float32 [2048], P('tp'), may hold values from 0.1 to 1.9
Outputs:
- result: bfloat16 [16384, 2048], P(('grp', 'fs'), 'tp'), parts along dimension 0
There are 2 independent parts, one for each index of `grp`. A program takes and returns all parts, laid end to end along the dimension named above; an argument that names none is the same for every part. Nothing has to cross between parts.
All inputs are finite; a program needn't handle non-finite values.
Results may differ from a plain program's by a relative error of at most 0.015.
Values may be sent and summed in bfloat16 or wider, within the bound.
A program may use at most 64 MiB of HBM per device.

v0:
```python
import jax
import jax.numpy as jnp
from jax import lax
from jax.sharding import PartitionSpec as P

D = 2048
DK = 128
DV = 256
BLOCK = 64
epsilon = 1e-06
highest = lax.Precision.HIGHEST


def copy_for_each(x, axis):
    copies = jnp.broadcast_to(x, (lax.axis_size(axis), *x.shape))
    return lax.all_to_all(copies, axis, split_axis=0, concat_axis=0, tiled=True)


def laid_out(blocks, dim):
    blocks = jnp.moveaxis(blocks, 0, dim)
    shape = blocks.shape
    return blocks.reshape(*shape[:dim], shape[dim] * shape[dim + 1], *shape[dim + 2 :])


def gather_directly(x, axis, dim):
    blocks = copy_for_each(x, axis)
    return laid_out(blocks, dim)


def side_by_side(arrays, axis, dim, along):
    ends, at = ([], 0)
    for a in arrays[:-1]:
        at += a.shape[along]
        ends.append(at)
    both = jnp.concatenate(arrays, axis=along)
    return tuple(jnp.split(lax.all_gather(both, axis, axis=dim, tiled=True), ends, axis=along))


def in_blocks(x, dim, devices):
    before, after = (x.shape[:dim], x.shape[dim + 1 :])
    return jnp.moveaxis(x.reshape(*before, devices, -1, *after), dim, 0)


def summed_on_arrival(x, axis, dim):
    blocks = in_blocks(x, dim, lax.axis_size(axis))
    arrived = lax.all_to_all(blocks, axis, split_axis=0, concat_axis=0, tiled=True)
    return arrived.astype(jnp.float32).sum(axis=0)


def over_copies(x, axis):
    everything = copy_for_each(x, axis)
    return jnp.sum(everything, axis=0)


def rms_rows(values, gain):
    values = values.astype(jnp.float32)
    factor = lax.rsqrt(jnp.mean(values * values, axis=-1, keepdims=True) + epsilon)
    return values * factor * gain


def blockwise_gla(query_rows, key_rows, value_rows, log_decay, head_count):
    length = query_rows.shape[0]
    blocks = length // BLOCK

    def split_heads(array, depth):
        return (
            array.astype(jnp.float32)
            .reshape(blocks, BLOCK, head_count, depth)
            .transpose(2, 0, 1, 3)
        )

    query_f = split_heads(query_rows, DK) * DK ** (-0.5)
    key_f = split_heads(key_rows, DK)
    value_f = split_heads(value_rows, DV)
    log_cum = jnp.cumsum(split_heads(log_decay, DK), axis=2)
    log_last = log_cum[:, :, -1:, :]
    query_dec = query_f * jnp.exp(log_cum)
    key_dec = key_f * jnp.exp(-log_cum)
    causal = jnp.tril(jnp.ones((BLOCK, BLOCK), dtype=bool))
    scores = jnp.where(
        causal, jnp.einsum("hncd,hnsd->hncs", query_dec, key_dec, precision=highest), 0.0
    )
    inside = jnp.einsum("hncs,hnsv->hncv", scores, value_f, precision=highest)
    contrib = jnp.einsum(
        "hncd,hncv->hndv", key_f * jnp.exp(log_last - log_cum), value_f, precision=highest
    )
    decay_block = jnp.exp(log_last[:, :, 0, :])

    def advance(carry_state, inputs):
        decay_step, added = inputs
        return (decay_step[..., None] * carry_state + added, carry_state)

    start_state = jnp.zeros((head_count, DK, DV), jnp.float32)
    final_state, earlier = lax.scan(
        advance, start_state, (jnp.moveaxis(decay_block, 1, 0), jnp.moveaxis(contrib, 1, 0))
    )
    earlier = jnp.moveaxis(earlier, 0, 1)
    output = inside + jnp.einsum("hncd,hndv->hncv", query_dec, earlier, precision=highest)
    return output.transpose(1, 2, 0, 3).reshape(length, head_count, DV)


def body(
    tokens,
    attn_gain,
    w_query,
    w_key,
    w_value,
    w_low,
    w_lift,
    decay_bias,
    head_gain,
    w_out,
    ffn_gain,
    w_gate,
    w_up,
    w_down,
    final_gain,
):
    row_count = tokens.shape[0]
    whole_rows = gather_directly(tokens, "tp", 1)
    normed = rms_rows(whole_rows, attn_gain).astype(jnp.bfloat16)

    def add_pieces(source, pieces):
        return tuple(
            (
                jnp.dot(source, weight_piece, preferred_element_type=jnp.float32)
                for weight_piece in pieces
            )
        )

    query_sum, key_sum, value_sum = add_pieces(
        normed, side_by_side((w_query, w_key, w_value), "fs", 0, 1)
    )
    query_rows = query_sum.astype(jnp.bfloat16)
    key_rows = key_sum.astype(jnp.bfloat16)
    value_rows = value_sum.astype(jnp.bfloat16)
    low_rank = jnp.dot(normed, w_low, preferred_element_type=jnp.float32).astype(jnp.bfloat16)
    log_decay = (
        jax.nn.log_sigmoid(
            jnp.dot(low_rank, w_lift, preferred_element_type=jnp.float32) + decay_bias
        )
        / 16.0
    )
    head_count = query_rows.shape[1] // DK
    gla_out = blockwise_gla(query_rows, key_rows, value_rows, log_decay, head_count)
    mixed_heads = (
        rms_rows(gla_out, head_gain).reshape(row_count, head_count * DV).astype(jnp.bfloat16)
    )
    out_terms = jnp.dot(
        mixed_heads, gather_directly(w_out, "fs", 1), preferred_element_type=jnp.float32
    )
    own_sum = summed_on_arrival(out_terms.astype(jnp.bfloat16), "tp", 1)
    first_sum = (tokens.astype(jnp.float32) + own_sum).astype(jnp.bfloat16)
    full_rows = gather_directly(first_sum, "tp", 1)
    normed_ffn = rms_rows(full_rows, ffn_gain).astype(jnp.bfloat16)
    gate_rows, up_rows = add_pieces(normed_ffn, side_by_side((w_gate, w_up), "fs", 0, 1))
    hidden = (jax.nn.silu(gate_rows) * up_rows).astype(jnp.bfloat16)
    down_terms = jnp.dot(
        hidden, lax.all_gather(w_down, "fs", axis=1, tiled=True), preferred_element_type=jnp.float32
    )
    own_ffn = summed_on_arrival(down_terms.astype(jnp.bfloat16), "tp", 1)
    second_sum = first_sum.astype(jnp.float32) + own_ffn
    square_sum = over_copies(jnp.sum(second_sum * second_sum, axis=1), "tp")
    factor = lax.rsqrt(square_sum / D + epsilon)[:, None]
    return (second_sum * factor * final_gain).astype(jnp.bfloat16)


def solution(mesh):
    return jax.shard_map(
        body,
        mesh=mesh,
        in_specs=(
            P(("grp", "fs"), "tp"),
            P(),
            P("fs", "tp"),
            P("fs", "tp"),
            P("fs", "tp"),
            P(),
            P(None, "tp"),
            P("tp"),
            P(),
            P("tp", "fs"),
            P(),
            P("fs", "tp"),
            P("fs", "tp"),
            P("tp", "fs"),
            P("tp"),
        ),
        out_specs=P(("grp", "fs"), "tp"),
        check_vma=False,
    )
```

profile of v0, /device:TPU:33, one launch (start us, length us, event | category | flops | bytes accessed | tf_op | source)
XLA Modules:
  0.0 365.1 jit_solution(1852456690066622126)
XLA Ops:
  6.6 1.6 pad_maximum_fusion.1
  8.2 1.1 copy.65
  9.3 1.6 broadcast_in_dim.44
  10.8 24.1 %all-to-all-start = ((bf16[8,512,256]{1,2,0:T(8,128)(2,1)}), bf16[8,512,256]{1,2,0:T(8,128)(2,1)S(1)}, u32[]{:S(2)}, u32[]{:S(2)}) async-start(bf16[8,512,256]{1,2,0:T(8,128)(2,1)} %broadcast_in_dim.44), calls=%async_computation | async-start | bytes 4194304 | tf_op jit(solution)/shard_map/all_to_all | solution.py:16
  34.9 0.8 pad_maximum_fusion
  35.9 25.3 %all-to-all-done = bf16[8,512,256]{1,2,0:T(8,128)(2,1)S(1)} async-done(((bf16[8,512,256]{1,2,0:T(8,128)(2,1)}), bf16[8,512,256]{1,2,0:T(8,128)(2,1)S(1)}, u32[]{:S(2)}, u32[]{:S(2)}) %all-to-all-start) | async-done | bytes 2097184 | tf_op jit(solution)/shard_map/all_to_all | solution.py:16
  61.2 1.1 broadcast_in_dim.48
  62.3 5.8 %all-to-all-start.1 = ((bf16[16,256,128]{1,2,0:T(8,128)(2,1)}), bf16[16,256,128]{1,2,0:T(8,128)(2,1)S(1)}, u32[]{:S(2)}, u32[]{:S(2)}) async-start(bf16[16,256,128]{1,2,0:T(8,128)(2,1)} %broadcast_in_dim.48), calls=%async_computation.1 | async-start | bytes 2097152 | tf_op jit(solution)/shard_map/all_to_all | solution.py:16
  68.1 0.5 multiply_reduce_fusion.1
  68.6 1.9 fusion.4
  70.6 3.2 fusion.28
  73.8 1.1 fusion.36
  74.9 0.7 copy-done.5
  75.6 39.5 %all-gather.4.cloned.1.call-done = bf16[2048,512]{1,0:T(8,128)(2,1)} async-done(((bf16[128,512]{1,0:T(8,128)(2,1)}), bf16[2048,512]{1,0:T(8,128)(2,1)}) %all-gather.4.cloned.1.call-update) | async-done | bytes 2097168 | tf_op jit(solution)/shard_map/all_gather | solution.py:36
  115.2 1.9 convolution_convert_fusion.3
  117.2 0.7 fusion.17
  118.1 0.3 fusion.33
  118.4 0.8 convolution_convert_fusion.2
  119.2 0.6 convolution_bitcast_fusion
  119.8 0.6 convolution_select_fusion
  120.4 0.4 fusion.43
  120.8 6.2 %while.13 = (s32[]{:T(128)}, f32[1,128,256]{2,1,0:T(8,128)S(1)}, f32[8,1,128,256]{3,2,1,0:T(8,128)}, f32[8,1,128]{2,1,0:T(1,128)S(1)}, f32[8,1,128,256]{3,2,1,0:T(8,128)S(1)}, /*index=5*/s32[]{:T(128)}, s32[]{:T(128)}) while((s32[]{:T(128)}, f32[1,128,256]{2,1,0:T(8,128)S(1)}, f32[8,1,128,256]{3,2,1,0:T(8,128)}, ...), condition=%wide.region_3.4_spmd.clone, body=%wide.region_2.3_spmd.clone.sunk | while | flops 131075 | bytes 657504 | solution.py:94
  120.8 0.7 bitcast_dynamic-update-slice_fusion.2
  121.6 0.7 bitcast_dynamic-update-slice_fusion.2
  122.4 0.7 bitcast_dynamic-update-slice_fusion.2
  123.2 0.7 bitcast_dynamic-update-slice_fusion.2
  123.9 0.6 bitcast_dynamic-update-slice_fusion.2
  124.7 0.7 bitcast_dynamic-update-slice_fusion.2
  125.5 0.7 bitcast_dynamic-update-slice_fusion.2
  126.3 0.7 bitcast_dynamic-update-slice_fusion.2
  127.1 2.0 multiply_reduce_fusion.3
  129.2 0.8 convolution_convert_fusion
  130.0 1.5 copy.102
  131.5 16.1 %all-to-all-start.2 = ((bf16[8,512,256]{2,1,0:T(8,128)(2,1)}), bf16[8,512,256]{2,1,0:T(8,128)(2,1)S(1)}, u32[]{:S(2)}, u32[]{:S(2)}) async-start(bf16[8,512,256]{2,1,0:T(8,128)(2,1)} %bitcast.95), calls=%async_computation.2 | async-start | bytes 4194304 | tf_op jit(solution)/shard_map/all_to_all | solution.py:46
  147.6 0.7 all-gather.8.cloned.1.call-update
  148.3 25.4 %all-to-all-done.2 = bf16[8,512,256]{2,1,0:T(8,128)(2,1)S(1)} async-done(((bf16[8,512,256]{2,1,0:T(8,128)(2,1)}), bf16[8,512,256]{2,1,0:T(8,128)(2,1)S(1)}, u32[]{:S(2)}, u32[]{:S(2)}) %all-to-all-start.2) | async-done | bytes 2097184 | tf_op jit(solution)/shard_map/all_to_all | solution.py:46
  173.8 0.3 convert_reduce_fusion.1
  174.5 29.7 %all_to_all.31 = bf16[8,512,256]{1,2,0:T(8,128)(2,1)S(1)} all-to-all(bf16[8,512,256]{1,2,0:T(8,128)(2,1)S(1)} %broadcast_in_dim.49), channel_id=1, replica_groups=mesh['grp'=2,'fs'=16,'tp'=8] {'tp'}, dimensions={0} | all-to-all | bytes 4194304 | tf_op jit(solution)/shard_map/all_to_all | solution.py:16
  204.2 0.5 multiply_reduce_fusion
  204.8 0.5 fusion.2
  205.4 15.2 %all-gather.6.cloned.1.call-done = bf16[2048,1408]{0,1:T(8,128)(2,1)} async-done(((bf16[128,1408]{0,1:T(8,128)(2,1)}), bf16[2048,1408]{0,1:T(8,128)(2,1)}) %all-gather.6.cloned.1.call-update) | async-done | bytes 5767184 | tf_op jit(solution)/shard_map/all_gather | solution.py:36
  220.6 4.6 %fusion.7 = f32[512,704]{0,1:T(8,128)} fusion(bf16[512,2048]{0,1:T(8,128)(2,1)S(1)} %fusion.2, bf16[2048,1408]{0,1:T(8,128)(2,1)} %all-gather.6.cloned.1.call-done), kind=kOutput, calls=%fused_computation.18 | convolution fusion | flops 1476395008 | bytes 6422528 | tf_op jit(solution)/shard_map/dot_general | solution.py:126
  225.2 75.2 %all-gather.8.cloned.1.call-done = bf16[704,2048]{1,0:T(8,128)(2,1)} async-done(((bf16[704,128]{1,0:T(8,128)(2,1)}), bf16[704,2048]{1,0:T(8,128)(2,1)}) %all-gather.8.cloned.1.call-update) | async-done | bytes 2883600 | tf_op jit(solution)/shard_map/all_gather | solution.py:159
  300.3 7.1 %convolution_convert_fusion.1 = bf16[512,2048]{1,0:T(8,128)(2,1)S(1)} fusion(bf16[704,2048]{1,0:T(8,128)(2,1)} %all-gather.8.cloned.1.call-done, bf16[512,2048]{0,1:T(8,128)(2,1)} %copy-done.4, bf16[2048,1408]{0,1:T(8,128)(2,1)} %all-gather.6.cloned.1.call-done, f32[512,704]{0,1:T(8,128)} %fusion.7), kind=kOutput, calls=%fused_computation.15 | convolution fusion | flops 2956001280 | bytes 11403264 | tf_op jit(solution)/shard_map/dot_general | solution.py:158
  307.6 41.4 %all_to_all.32 = bf16[8,512,256]{2,1,0:T(8,128)(2,1)S(1)} all-to-all(bf16[8,512,256]{2,1,0:T(8,128)(2,1)S(1)} %bitcast.97), channel_id=1, replica_groups=mesh['grp'=2,'fs'=16,'tp'=8] {'tp'}, dimensions={0} | all-to-all | bytes 4194304 | tf_op jit(solution)/shard_map/all_to_all | solution.py:46
  349.1 0.3 convert_reduce_fusion
  349.5 8.1 %all_to_all.33 = f32[8,1,512]{2,1,0:T(1,128)S(1)} all-to-all(f32[8,1,512]{2,1,0:T(1,128)S(1)} %broadcast_in_dim.50), channel_id=1, replica_groups=mesh['grp'=2,'fs'=16,'tp'=8] {'tp'}, dimensions={0} | all-to-all | bytes 32768 | tf_op jit(solution)/shard_map/all_to_all | solution.py:16
  357.7 0.8 multiply_convert_fusion
  (75 shorter events, 2.2 us)
Async XLA Ops:
  6.5 64.0 %copy-start = (bf16[2048,32]{0,1:T(8,128)(2,1)S(1)}, bf16[2048,32]{0,1:T(8,128)(2,1)}, u32[]{:S(2)}) copy-start(bf16[2048,32]{0,1:T(8,128)(2,1)} %param.22) | copy-start | bytes 393220
  6.6 108.6 %all-gather.4.cloned.1.call-start = ((), (), s32[]{:S(2)}) async-start(), calls=%async_computation.6 | async-start | bytes 2228224 | tf_op jit(solution)/shard_map/all_gather | solution.py:36
  10.8 24.1 %copy-start.8 = (bf16[128,704]{0,1:T(8,128)(2,1)S(1)}, bf16[128,704]{0,1:T(8,128)(2,1)}, u32[]{:S(2)}) copy-start(bf16[128,704]{0,1:T(8,128)(2,1)} %param.29) | copy-start | bytes 540676
  10.8 24.1 %copy-start.9 = (bf16[128,704]{0,1:T(8,128)(2,1)S(1)}, bf16[128,704]{0,1:T(8,128)(2,1)}, u32[]{:S(2)}) copy-start(bf16[128,704]{0,1:T(8,128)(2,1)} %param.28) | copy-start | bytes 540676
  10.8 24.9 %copy-start.10 = (bf16[256,128]{1,0:T(8,128)(2,1)S(1)}, bf16[256,128]{1,0:T(8,128)(2,1)}, u32[]{:S(2)}) copy-start(bf16[256,128]{1,0:T(8,128)(2,1)} %param.26) | copy-start | bytes 196612
  10.8 50.4 %all-to-all-start = ((bf16[8,512,256]{1,2,0:T(8,128)(2,1)}), bf16[8,512,256]{1,2,0:T(8,128)(2,1)S(1)}, u32[]{:S(2)}, u32[]{:S(2)}) async-start(bf16[8,512,256]{1,2,0:T(8,128)(2,1)} %broadcast_in_dim.44), calls=%async_computation | async-start | bytes 4194304 | tf_op jit(solution)/shard_map/all_to_all | solution.py:16
  34.9 185.7 %all-gather.6.cloned.1.call-start = ((), (), s32[]{:S(2)}) async-start(), calls=%async_computation.7 | async-start | bytes 6127616 | tf_op jit(solution)/shard_map/all_gather | solution.py:36
  62.3 6.3 %copy-start.11 = (f32[2048]{0:T(1024)S(1)}, f32[2048]{0:T(1024)}, u32[]{:S(2)}) copy-start(f32[2048]{0:T(1024)} %param.18) | copy-start | bytes 24580
  62.3 66.9 %all-to-all-start.1 = ((bf16[16,256,128]{1,2,0:T(8,128)(2,1)}), bf16[16,256,128]{1,2,0:T(8,128)(2,1)S(1)}, u32[]{:S(2)}, u32[]{:S(2)}) async-start(bf16[16,256,128]{1,2,0:T(8,128)(2,1)} %broadcast_in_dim.48), calls=%async_computation.1 | async-start | bytes 2097152 | tf_op jit(solution)/shard_map/all_to_all | solution.py:16
  68.6 2.0 copy-start.12
  68.6 1.9 copy-start.16
  70.6 44.6 %copy-start.1 = (bf16[512,2048]{0,1:T(8,128)(2,1)S(1)}, bf16[512,2048]{0,1:T(8,128)(2,1)}, u32[]{:S(2)}) copy-start(bf16[512,2048]{0,1:T(8,128)(2,1)} %fusion.4) | copy-start | bytes 6291460
  74.9 0.7 copy-start.5
  115.2 2.0 copy-start.17
  117.1 1.0 copy-start.6
  118.4 1.4 copy-start.2
  120.4 6.6 %copy-start.3 = (f32[8,64,128]{2,0,1:T(8,128)S(1)}, f32[8,64,128]{2,0,1:T(8,128)}, u32[]{:S(2)}) copy-start(f32[8,64,128]{2,0,1:T(8,128)} %copy-done.2) | copy-start | bytes 786436
  120.8 8.4 %copy-start.15 = (f32[256]{0:T(256)S(1)}, f32[256]{0:T(256)}, u32[]{:S(2)}) copy-start(f32[256]{0:T(256)} %param.25) | copy-start | bytes 3076
  131.5 42.3 %all-to-all-start.2 = ((bf16[8,512,256]{2,1,0:T(8,128)(2,1)}), bf16[8,512,256]{2,1,0:T(8,128)(2,1)S(1)}, u32[]{:S(2)}, u32[]{:S(2)}) async-start(bf16[8,512,256]{2,1,0:T(8,128)(2,1)} %bitcast.95), calls=%async_computation.2 | async-start | bytes 4194304 | tf_op jit(solution)/shard_map/all_to_all | solution.py:46
  147.6 26.5 %copy-start.7 = (bf16[512,256]{1,0:T(8,128)(2,1)S(1)}, bf16[512,256]{1,0:T(8,128)(2,1)}, u32[]{:S(2)}) copy-start(bf16[512,256]{1,0:T(8,128)(2,1)} %param.17) | copy-start | bytes 786436
  147.6 152.7 %all-gather.8.cloned.1.call-start = ((), (), s32[]{:S(2)}) async-start(), calls=%async_computation.8 | async-start | bytes 3063808 | tf_op jit(solution)/shard_map/all_gather | solution.py:159
  204.1 0.7 copy-start.13
  205.4 19.8 %copy-start.4 = (bf16[512,2048]{0,1:T(8,128)(2,1)}, bf16[512,2048]{0,1:T(8,128)(2,1)S(1)}, u32[]{:S(2)}) copy-start(bf16[512,2048]{0,1:T(8,128)(2,1)S(1)} %fusion.2) | copy-start | bytes 6291460
  349.1 8.6 %copy-start.14 = (f32[256]{0:T(256)S(1)}, f32[256]{0:T(256)}, u32[]{:S(2)}) copy-start(f32[256]{0:T(256)} %param.31) | copy-start | bytes 3076
Sparse Core Ops, SparseCore 0:
  9.1 105.9 all-gather.3
  116.9 103.6 all-gather.5
  222.3 77.9 all-gather.7
where the time goes:
time: 366 us; the launch traced here: 365 us
  waiting for transfers between devices  181 us (49%)
  blocking collectives  79.2 us (22%)
  starting transfers between devices  46 us (13%)
  matrix products  22.7 us (6%)
  other arithmetic  15 us (4%)
  between operations  13.4 us (4%)
  local copies, waits for them, and re-layouts  7 us (2%)
    all_gather x1, waiting for transfers between devices, body(): lax.all_gather(w_down, 'fs', axis=1, tiled=True)  75.2 us
    all_gather x2, waiting for transfers between devices, side_by_side(): lax.all_gather(both, axis, axis=dim, tiled=True)  54.7 us
    all_to_all x1, blocking collectives, summed_on_arrival(): lax.all_to_all(blocks, axis, split_axis=0, concat_axis=0, tiled=True)  41.4 us
    all_to_all x2, blocking collectives, copy_for_each(): return lax.all_to_all(copies, axis, split_axis=0, concat_axis=0, tiled=True)  37.8 us
    all_to_all x2, starting transfers between devices, copy_for_each(): return lax.all_to_all(copies, axis, split_axis=0, concat_axis=0, tiled=True)  29.9 us
    all_to_all x1, waiting for transfers between devices, summed_on_arrival(): lax.all_to_all(blocks, axis, split_axis=0, concat_axis=0, tiled=True)  25.4 us
    all_to_all x2, waiting for transfers between devices, copy_for_each(): return lax.all_to_all(copies, axis, split_axis=0, concat_axis=0, tiled=True)  25.3 us
    all_to_all x1, starting transfers between devices, summed_on_arrival(): lax.all_to_all(blocks, axis, split_axis=0, concat_axis=0, tiled=True)  16.1 us
  transfers between devices with their start and end apart: 6, of which 5 were waited for; matrix products, arithmetic and copies ran while one was open for 9% of the time, Pallas kernels for 0%

commit v1 on v0

--- a/solution.py
+++ b/solution.py
@@ -9,6 +9,28 @@
 BLOCK = 64
 epsilon = 1e-06
 highest = lax.Precision.HIGHEST
+
+
+def in_order(parts, dim):
+    shape = list(parts.shape[1:])
+    shape[dim] *= parts.shape[0]
+    return jnp.moveaxis(parts, 0, dim).reshape(shape)
+
+
+def ring_gather(shard, axis, dim):
+    size = lax.axis_size(axis)
+    pairs = [(i, (i + 1) % size) for i in range(size)]
+    back = [(b, a) for a, b in pairs]
+    lower, upper = ([], [])
+    for turn in range(size - 1):
+        if turn % 2 == 0:
+            lower.append(lax.ppermute(lower[-1] if lower else shard, axis, pairs))
+        else:
+            upper.append(lax.ppermute(upper[-1] if upper else shard, axis, back))
+    blocks = jnp.stack([*lower[::-1], shard, *upper])
+    shift = lax.axis_index(axis) - len(lower)
+    blocks = blocks[(jnp.arange(size) - shift) % size]
+    return in_order(blocks, dim)
 
 
 def copy_for_each(x, axis):
@@ -155,9 +177,7 @@
     normed_ffn = rms_rows(full_rows, ffn_gain).astype(jnp.bfloat16)
     gate_rows, up_rows = add_pieces(normed_ffn, side_by_side((w_gate, w_up), "fs", 0, 1))
     hidden = (jax.nn.silu(gate_rows) * up_rows).astype(jnp.bfloat16)
-    down_terms = jnp.dot(
-        hidden, lax.all_gather(w_down, "fs", axis=1, tiled=True), preferred_element_type=jnp.float32
-    )
+    down_terms = jnp.dot(hidden, ring_gather(w_down, "fs", 1), preferred_element_type=jnp.float32)
     own_ffn = summed_on_arrival(down_terms.astype(jnp.bfloat16), "tp", 1)
     second_sum = first_sum.astype(jnp.float32) + own_ffn
     square_sum = over_copies(jnp.sum(second_sum * second_sum, axis=1), "tp")

time: 366 us -> 294 us (0.80)
  waiting for transfers between devices: 181 us -> 82.4 us
  blocking collectives: 79.2 us -> 44.4 us
  starting transfers between devices: 46 us -> 80.8 us
  local copies, waits for them, and re-layouts: 7 us -> 31.9 us
    all_gather x1 -> x0, waiting for transfers between devices: 75.2 us -> none  [body(): lax.all_gather(w_down, 'fs', axis=1, tiled=True)]
    all_gather x2, waiting for transfers between devices: 54.7 us -> 0.01 us  [side_by_side(): lax.all_gather(both, axis, axis=dim, tiled=True)]
    all_to_all x2 -> x1, blocking collectives: 37.8 us -> 8.11 us  [copy_for_each(): return lax.all_to_all(copies, axis, split_axis=0, concat_axis=0, tiled=True)]
    ppermute x0 -> x15, waiting for transfers between devices: none -> 27.6 us  [the longest x8 25.1 us: ring_gather(): lower.append(lax.ppermute(lower[-1] if lower else shard, axis, pairs))]
    ppermute x0 -> x15, starting transfers between devices: none -> 23.9 us  [the longest x7 22.8 us: ring_gather(): upper.append(lax.ppermute(upper[-1] if upper else shard, axis, back))]
    unnamed x38 -> x93, local copies, waits for them, and re-layouts: 2.3 us -> 19.9 us
    all_to_all x2 -> x3, waiting for transfers between devices: 25.3 us -> 36.7 us  [copy_for_each(): return lax.all_to_all(copies, axis, split_axis=0, concat_axis=0, tiled=True)]
    all_to_all x1, waiting for transfers between devices: 25.4 us -> 17.9 us  [summed_on_arrival(): lax.all_to_all(blocks, axis, split_axis=0, concat_axis=0, tiled=True)]
  transfers between devices with their start and end apart: 6 -> 21, of which waited for: 5 -> 12; matrix products, arithmetic and copies ran while one was open for 9% -> 18% of each run, Pallas kernels for 0% -> 0%
where the time goes in v1:
time: 294 us; the launch traced here: 293 us
  waiting for transfers between devices  82.4 us (28%)
  starting transfers between devices  80.8 us (27%)
  blocking collectives  44.4 us (15%)
  local copies, waits for them, and re-layouts  31.9 us (11%)
  matrix products  23.4 us (8%)
  other arithmetic  16.3 us (6%)
  between operations  13.9 us (5%)
    all_to_all x3, starting transfers between devices, copy_for_each(): return lax.all_to_all(copies, axis, split_axis=0, concat_axis=0, tiled=True)  37.3 us
    all_to_all x3, waiting for transfers between devices, copy_for_each(): return lax.all_to_all(copies, axis, split_axis=0, concat_axis=0, tiled=True)  36.7 us
    all_to_all x1, blocking collectives, summed_on_arrival(): lax.all_to_all(blocks, axis, split_axis=0, concat_axis=0, tiled=True)  36.3 us
    ppermute x8, waiting for transfers between devices, ring_gather(): lower.append(lax.ppermute(lower[-1] if lower else shard, axis, pairs))  25.1 us
    ppermute x7, starting transfers between devices, ring_gather(): upper.append(lax.ppermute(upper[-1] if upper else shard, axis, back))  22.8 us
    unnamed x93, local copies, waits for them, and re-layouts  19.9 us
    all_to_all x1, starting transfers between devices, summed_on_arrival(): lax.all_to_all(blocks, axis, split_axis=0, concat_axis=0, tiled=True)  19.7 us
    all_to_all x1, waiting for transfers between devices, summed_on_arrival(): lax.all_to_all(blocks, axis, split_axis=0, concat_axis=0, tiled=True)  17.9 us
  transfers between devices with their start and end apart: 21, of which 12 were waited for; matrix products, arithmetic and copies ran while one was open for 18% of the time, Pallas kernels for 0%

profile of v1, /device:TPU:33, one launch (start us, length us, event | category | flops | bytes accessed | tf_op | source)
XLA Modules:
  0.0 293.4 jit_solution(3714022552702939653)
XLA Ops:
  6.6 1.6 pad_maximum_fusion.1
  8.2 1.1 copy.68
  9.3 1.6 broadcast_in_dim.45
  10.9 23.9 %all-to-all-start = ((bf16[8,512,256]{1,2,0:T(8,128)(2,1)}), bf16[8,512,256]{1,2,0:T(8,128)(2,1)S(1)}, u32[]{:S(2)}, u32[]{:S(2)}) async-start(bf16[8,512,256]{1,2,0:T(8,128)(2,1)} %broadcast_in_dim.45), calls=%async_computation | async-start | bytes 4194304 | tf_op jit(solution)/shard_map/all_to_all | solution.py:38
  34.9 4.3 %collective-permute-start.8 = (bf16[704,128]{1,0:T(8,128)(2,1)S(1)}, bf16[704,128]{1,0:T(8,128)(2,1)S(1)}, u32[]{:S(2)}, u32[]{:S(2)}) collective-permute-start(bf16[704,128]{1,0:T(8,128)(2,1)S(1)} %copy-done.7), channel_id=1, source_target_pairs={{8,0},{16,8},{24,16},{32,24},{40,32},{48,40},{56,48},{64,56},{72,6... | collective-permute-start | bytes 540680 | tf_op jit(solution)/shard_map/ppermute | solution.py:29
  39.2 5.9 %collective-permute-done = bf16[704,128]{1,0:T(8,128)(2,1)S(1)} collective-permute-done((bf16[704,128]{1,0:T(8,128)(2,1)S(1)}, bf16[704,128]{1,0:T(8,128)(2,1)S(1)}, u32[]{:S(2)}, u32[]{:S(2)}) %collective-permute-start) | collective-permute-done | bytes 180256 | tf_op jit(solution)/shard_map/ppermute | solution.py:27
  45.8 2.6 collective-permute-start.9
  48.4 5.0 %collective-permute-done.1 = bf16[704,128]{1,0:T(8,128)(2,1)S(1)} collective-permute-done((bf16[704,128]{1,0:T(8,128)(2,1)S(1)}, bf16[704,128]{1,0:T(8,128)(2,1)S(1)}, u32[]{:S(2)}, u32[]{:S(2)}) %collective-permute-start.1) | collective-permute-done | bytes 180256 | tf_op jit(solution)/shard_map/ppermute | solution.py:27
  54.7 3.5 %collective-permute-start.10 = (bf16[704,128]{1,0:T(8,128)(2,1)S(1)}, bf16[704,128]{1,0:T(8,128)(2,1)S(1)}, u32[]{:S(2)}, u32[]{:S(2)}) collective-permute-start(bf16[704,128]{1,0:T(8,128)(2,1)S(1)} %collective-permute-done.9), channel_id=1, source_target_pairs={{8,0},{16,8},{24,16},{32,24},{40,32},{48,40},{56,48},{64,56},{72,6... | collective-permute-start | bytes 540680 | tf_op jit(solution)/shard_map/ppermute | solution.py:29
  58.2 2.6 collective-permute-done.2
  61.7 3.0 %collective-permute-start.11 = (bf16[704,128]{1,0:T(8,128)(2,1)S(1)}, bf16[704,128]{1,0:T(8,128)(2,1)S(1)}, u32[]{:S(2)}, u32[]{:S(2)}) collective-permute-start(bf16[704,128]{1,0:T(8,128)(2,1)S(1)} %collective-permute-done.10), channel_id=1, source_target_pairs={{8,0},{16,8},{24,16},{32,24},{40,32},{48,40},{56,48},{64,56},{72,6... | collective-permute-start | bytes 540680 | tf_op jit(solution)/shard_map/ppermute | solution.py:29
  64.6 3.6 %collective-permute-done.3 = bf16[704,128]{1,0:T(8,128)(2,1)S(1)} collective-permute-done((bf16[704,128]{1,0:T(8,128)(2,1)S(1)}, bf16[704,128]{1,0:T(8,128)(2,1)S(1)}, u32[]{:S(2)}, u32[]{:S(2)}) %collective-permute-start.3) | collective-permute-done | bytes 180256 | tf_op jit(solution)/shard_map/ppermute | solution.py:27
  68.3 3.1 %collective-permute-start.12 = (bf16[704,128]{1,0:T(8,128)(2,1)S(1)}, bf16[704,128]{1,0:T(8,128)(2,1)S(1)}, u32[]{:S(2)}, u32[]{:S(2)}) collective-permute-start(bf16[704,128]{1,0:T(8,128)(2,1)S(1)} %collective-permute-done.11), channel_id=1, source_target_pairs={{8,0},{16,8},{24,16},{32,24},{40,32},{48,40},{56,48},{64,56},{72,6... | collective-permute-start | bytes 540680 | tf_op jit(solution)/shard_map/ppermute | solution.py:29
  71.4 4.1 %collective-permute-done.4 = bf16[704,128]{1,0:T(8,128)(2,1)S(1)} collective-permute-done((bf16[704,128]{1,0:T(8,128)(2,1)S(1)}, bf16[704,128]{1,0:T(8,128)(2,1)S(1)}, u32[]{:S(2)}, u32[]{:S(2)}) %collective-permute-start.4) | collective-permute-done | bytes 180256 | tf_op jit(solution)/shard_map/ppermute | solution.py:27
  76.3 0.9 copy.79
  77.3 2.8 collective-permute-start.13
  80.1 2.6 collective-permute-done.5
  82.7 1.9 collective-permute-done.13
  84.6 3.6 %collective-permute-start.14 = (bf16[704,128]{1,0:T(8,128)(2,1)}, bf16[704,128]{1,0:T(8,128)(2,1)}, u32[]{:S(2)}, u32[]{:S(2)}) collective-permute-start(bf16[704,128]{1,0:T(8,128)(2,1)} %collective-permute-done.13), channel_id=1, source_target_pairs={{8,0},{16,8},{24,16},{32,24},{40,32},{48,40},{56,48},{64,56},{72,6... | collective-permute-start | bytes 540680 | tf_op jit(solution)/shard_map/ppermute | solution.py:29
  88.2 1.5 collective-permute-done.6
  89.6 1.1 broadcast_in_dim.49
  90.7 8.7 %all-to-all-start.1 = ((bf16[16,256,128]{1,2,0:T(8,128)(2,1)}), bf16[16,256,128]{1,2,0:T(8,128)(2,1)S(1)}, u32[]{:S(2)}, u32[]{:S(2)}) async-start(bf16[16,256,128]{1,2,0:T(8,128)(2,1)} %broadcast_in_dim.49), calls=%async_computation.1 | async-start | bytes 2097152 | tf_op jit(solution)/shard_map/all_to_all | solution.py:38
  100.0 1.9 fusion.4
  101.9 3.2 %fusion.30 = f32[512,128]{1,0:T(8,128)} fusion(bf16[32,128]{1,0:T(8,128)(2,1)S(1)} %copy-done.32, bf16[2048,32]{0,1:T(8,128)(2,1)S(1)} %copy-done, bf16[512,2048]{0,1:T(8,128)(2,1)} %fusion.4, f32[128]{0:T(128)S(1)} %copy-done.36), kind=kOutput, calls=%fused_computation.53 | convolution fusion | flops 71974912 | bytes 2499072 | tf_op jit(solution)/shard_map/dot_general | solution.py:162
  105.1 1.1 fusion.38
  107.0 1.9 convolution_convert_fusion.3
  113.2 6.2 %while.13 = (s32[]{:T(128)}, f32[1,128,256]{2,1,0:T(8,128)S(1)}, f32[8,1,128,256]{3,2,1,0:T(8,128)}, f32[8,1,128]{2,1,0:T(1,128)S(1)}, f32[8,1,128,256]{3,2,1,0:T(8,128)S(1)}, /*index=5*/s32[]{:T(128)}, s32[]{:T(128)}) while((s32[]{:T(128)}, f32[1,128,256]{2,1,0:T(8,128)S(1)}, f32[8,1,128,256]{3,2,1,0:T(8,128)}, ...), condition=%wide.region_3.4_spmd.clone, body=%wide.region_2.3_spmd.clone.sunk | while | flops 131075 | bytes 657504 | solution.py:116
  119.4 2.0 multiply_reduce_fusion.3
  121.5 23.1 %all-to-all-done.1 = bf16[16,256,128]{1,2,0:T(8,128)(2,1)S(1)} async-done(((bf16[16,256,128]{1,2,0:T(8,128)(2,1)}), bf16[16,256,128]{1,2,0:T(8,128)(2,1)S(1)}, u32[]{:S(2)}, u32[]{:S(2)}) %all-to-all-start.1) | async-done | bytes 1048608 | tf_op jit(solution)/shard_map/all_to_all | solution.py:38
  145.4 1.5 copy.111
  146.9 19.7 %all-to-all-start.2 = ((bf16[8,512,256]{2,1,0:T(8,128)(2,1)}), bf16[8,512,256]{2,1,0:T(8,128)(2,1)S(1)}, u32[]{:S(2)}, u32[]{:S(2)}) async-start(bf16[8,512,256]{2,1,0:T(8,128)(2,1)} %bitcast.136), calls=%async_computation.2 | async-start | bytes 4194304 | tf_op jit(solution)/shard_map/all_to_all | solution.py:68
  166.6 1.7 bitcast_dynamic-update-slice_fusion.16
  168.3 1.6 bitcast_dynamic-update-slice_fusion.15
  169.9 1.6 bitcast_dynamic-update-slice_fusion.14
  174.9 17.9 %all-to-all-done.2 = bf16[8,512,256]{2,1,0:T(8,128)(2,1)S(1)} async-done(((bf16[8,512,256]{2,1,0:T(8,128)(2,1)}), bf16[8,512,256]{2,1,0:T(8,128)(2,1)S(1)}, u32[]{:S(2)}, u32[]{:S(2)}) %all-to-all-start.2) | async-done | bytes 2097184 | tf_op jit(solution)/shard_map/all_to_all | solution.py:68
  193.3 1.5 broadcast_in_dim.50
  194.9 4.6 %all-to-all-start.3 = ((bf16[8,512,256]{1,2,0:T(8,128)(2,1)}), bf16[8,512,256]{1,2,0:T(8,128)(2,1)S(1)}, u32[]{:S(2)}, u32[]{:S(2)}) async-start(bf16[8,512,256]{1,2,0:T(8,128)(2,1)} %broadcast_in_dim.50), calls=%async_computation.3 | async-start | bytes 4194304 | tf_op jit(solution)/shard_map/all_to_all | solution.py:38
  203.0 1.6 bitcast_dynamic-update-slice_fusion.3
  204.6 1.6 bitcast_dynamic-update-slice_fusion.2
  206.2 1.6 bitcast_dynamic-update-slice_fusion.1
  207.8 4.4 %gather_fusion = bf16[16,704,128]{2,1,0:T(8,128)(2,1)} fusion(bf16[16,704,128]{2,1,0:T(8,128)(2,1)} %bitcast_dynamic-update-slice_fusion.1, s32[1024]{0:T(1024)S(1)} %pad_clamp_fusion), kind=kCustom, calls=%fused_computation | custom fusion | bytes 5767232 | tf_op jit(solution)/shard_map/gather | solution.py:32
  212.2 13.6 %all-to-all-done.3 = bf16[8,512,256]{1,2,0:T(8,128)(2,1)S(1)} async-done(((bf16[8,512,256]{1,2,0:T(8,128)(2,1)}), bf16[8,512,256]{1,2,0:T(8,128)(2,1)S(1)}, u32[]{:S(2)}, u32[]{:S(2)}) %all-to-all-start.3) | async-done | bytes 2097184 | tf_op jit(solution)/shard_map/all_to_all | solution.py:38
  226.3 1.9 fusion.2
  228.2 5.2 %fusion.9 = f32[512,704]{0,1:T(8,128)} fusion(bf16[512,2048]{0,1:T(8,128)(2,1)} %fusion.2, bf16[2048,1408]{0,1:T(8,128)(2,1)} %all-gather.5.cloned.1.call-done), kind=kOutput, calls=%fused_computation.21 | convolution fusion | flops 1476395008 | bytes 6422528 | tf_op jit(solution)/shard_map/dot_general | solution.py:148
  233.4 7.1 %convolution_convert_fusion.1 = bf16[512,2048]{1,0:T(8,128)(2,1)S(1)} fusion(bf16[512,2048]{0,1:T(8,128)(2,1)} %fusion.2, bf16[2048,1408]{0,1:T(8,128)(2,1)} %all-gather.5.cloned.1.call-done, f32[512,704]{0,1:T(8,128)} %fusion.9, bf16[16,704,128]{2,1,0:T(8,128)(2,1)} %gather_fusion), kind=kOutput, calls=%fused_computation.16 | convolution fusion | flops 2956001280 | bytes 11403264 | tf_op jit(solution)/shard_map/dot_general | solution.py:180
  240.7 36.3 %all_to_all.31 = bf16[8,512,256]{2,1,0:T(8,128)(2,1)S(1)} all-to-all(bf16[8,512,256]{2,1,0:T(8,128)(2,1)S(1)} %bitcast.138), channel_id=1, replica_groups=mesh['grp'=2,'fs'=16,'tp'=8] {'tp'}, dimensions={0} | all-to-all | bytes 4194304 | tf_op jit(solution)/shard_map/all_to_all | solution.py:68
  277.5 8.1 %all_to_all.32 = f32[8,1,512]{2,1,0:T(1,128)S(1)} all-to-all(f32[8,1,512]{2,1,0:T(1,128)S(1)} %broadcast_in_dim.51), channel_id=1, replica_groups=mesh['grp'=2,'fs'=16,'tp'=8] {'tp'}, dimensions={0} | all-to-all | bytes 32768 | tf_op jit(solution)/shard_map/all_to_all | solution.py:38
  285.7 0.8 multiply_convert_fusion
  (162 shorter events, 24.8 us)
Async XLA Ops:
  6.5 95.4 %copy-start = (bf16[2048,32]{0,1:T(8,128)(2,1)S(1)}, bf16[2048,32]{0,1:T(8,128)(2,1)}, u32[]{:S(2)}) copy-start(bf16[2048,32]{0,1:T(8,128)(2,1)} %param.22) | copy-start | bytes 393220
  6.6 100.4 %all-gather.3.cloned.1.call-start = ((), (), s32[]{:S(2)}) async-start(), calls=%async_computation.6 | async-start | bytes 2228224 | tf_op jit(solution)/shard_map/all_gather | solution.py:58
  9.3 25.5 %copy-start.7 = (bf16[704,128]{1,0:T(8,128)(2,1)S(1)}, bf16[704,128]{1,0:T(8,128)(2,1)}, u32[]{:S(2)}) copy-start(bf16[704,128]{1,0:T(8,128)(2,1)} %param.30) | copy-start | bytes 540676
  9.3 66.2 %copy-start.29 = (bf16[128,704]{0,1:T(8,128)(2,1)S(1)}, bf16[128,704]{0,1:T(8,128)(2,1)}, u32[]{:S(2)}) copy-start(bf16[128,704]{0,1:T(8,128)(2,1)} %param.29) | copy-start | bytes 540676
  9.3 66.2 %copy-start.30 = (bf16[128,704]{0,1:T(8,128)(2,1)S(1)}, bf16[128,704]{0,1:T(8,128)(2,1)}, u32[]{:S(2)}) copy-start(bf16[128,704]{0,1:T(8,128)(2,1)} %param.28) | copy-start | bytes 540676
  10.9 78.8 %all-to-all-start = ((bf16[8,512,256]{1,2,0:T(8,128)(2,1)}), bf16[8,512,256]{1,2,0:T(8,128)(2,1)S(1)}, u32[]{:S(2)}, u32[]{:S(2)}) async-start(bf16[8,512,256]{1,2,0:T(8,128)(2,1)} %broadcast_in_dim.45), calls=%async_computation | async-start | bytes 4194304 | tf_op jit(solution)/shard_map/all_to_all | solution.py:38
  34.8 193.4 %all-gather.5.cloned.1.call-start = ((), (), s32[]{:S(2)}) async-start(), calls=%async_computation.7 | async-start | bytes 6127616 | tf_op jit(solution)/shard_map/all_gather | solution.py:58
  34.8 10.3 %collective-permute-start = (bf16[704,128]{1,0:T(8,128)(2,1)S(1)}, bf16[704,128]{1,0:T(8,128)(2,1)S(1)}, u32[]{:S(2)}, u32[]{:S(2)}) collective-permute-start(bf16[704,128]{1,0:T(8,128)(2,1)S(1)} %copy-done.7), channel_id=1, source_target_pairs={{0,8},{8,16},{16,24},{24,32},{32,40},{40,48},{48,56},{56,64},{64,7... | collective-permute-start | bytes 540680 | tf_op jit(solution)/shard_map/ppermute | solution.py:27
  34.9 10.1 %collective-permute-start.8 = (bf16[704,128]{1,0:T(8,128)(2,1)S(1)}, bf16[704,128]{1,0:T(8,128)(2,1)S(1)}, u32[]{:S(2)}, u32[]{:S(2)}) collective-permute-start(bf16[704,128]{1,0:T(8,128)(2,1)S(1)} %copy-done.7), channel_id=1, source_target_pairs={{8,0},{16,8},{24,16},{32,24},{40,32},{48,40},{56,48},{64,56},{72,6... | collective-permute-start | bytes 540680 | tf_op jit(solution)/shard_map/ppermute | solution.py:29
  45.1 16.6 %copy-start.13 = (bf16[704,128]{1,0:T(8,128)(2,1)}, bf16[704,128]{1,0:T(8,128)(2,1)S(1)}, u32[]{:S(2)}) copy-start(bf16[704,128]{1,0:T(8,128)(2,1)S(1)} %collective-permute-done) | copy-start | bytes 540676
  45.1 8.3 %collective-permute-start.1 = (bf16[704,128]{1,0:T(8,128)(2,1)S(1)}, bf16[704,128]{1,0:T(8,128)(2,1)S(1)}, u32[]{:S(2)}, u32[]{:S(2)}) collective-permute-start(bf16[704,128]{1,0:T(8,128)(2,1)S(1)} %collective-permute-done), channel_id=1, source_target_pairs={{0,8},{8,16},{16,24},{24,32},{32,40},{40,48},{48,56},{56,64},{64,7... | collective-permute-start | bytes 540680 | tf_op jit(solution)/shard_map/ppermute | solution.py:27
  45.8 8.2 %collective-permute-start.9 = (bf16[704,128]{1,0:T(8,128)(2,1)S(1)}, bf16[704,128]{1,0:T(8,128)(2,1)S(1)}, u32[]{:S(2)}, u32[]{:S(2)}) collective-permute-start(bf16[704,128]{1,0:T(8,128)(2,1)S(1)} %collective-permute-done.8), channel_id=1, source_target_pairs={{8,0},{16,8},{24,16},{32,24},{40,32},{48,40},{56,48},{64,56},{72,6... | collective-permute-start | bytes 540680 | tf_op jit(solution)/shard_map/ppermute | solution.py:29
  53.4 14.9 %copy-start.17 = (bf16[704,128]{1,0:T(8,128)(2,1)}, bf16[704,128]{1,0:T(8,128)(2,1)S(1)}, u32[]{:S(2)}) copy-start(bf16[704,128]{1,0:T(8,128)(2,1)S(1)} %collective-permute-done.1) | copy-start | bytes 540676
  53.4 7.3 %collective-permute-start.2 = (bf16[704,128]{1,0:T(8,128)(2,1)S(1)}, bf16[704,128]{1,0:T(8,128)(2,1)S(1)}, u32[]{:S(2)}, u32[]{:S(2)}) collective-permute-start(bf16[704,128]{1,0:T(8,128)(2,1)S(1)} %collective-permute-done.1), channel_id=1, source_target_pairs={{0,8},{8,16},{16,24},{24,32},{32,40},{40,48},{48,56},{56,64},{64,7... | collective-permute-start | bytes 540680 | tf_op jit(solution)/shard_map/ppermute | solution.py:27
  54.7 7.0 %collective-permute-start.10 = (bf16[704,128]{1,0:T(8,128)(2,1)S(1)}, bf16[704,128]{1,0:T(8,128)(2,1)S(1)}, u32[]{:S(2)}, u32[]{:S(2)}) collective-permute-start(bf16[704,128]{1,0:T(8,128)(2,1)S(1)} %collective-permute-done.9), channel_id=1, source_target_pairs={{8,0},{16,8},{24,16},{32,24},{40,32},{48,40},{56,48},{64,56},{72,6... | collective-permute-start | bytes 540680 | tf_op jit(solution)/shard_map/ppermute | solution.py:29
  60.7 10.6 %copy-start.22 = (bf16[704,128]{1,0:T(8,128)(2,1)}, bf16[704,128]{1,0:T(8,128)(2,1)S(1)}, u32[]{:S(2)}) copy-start(bf16[704,128]{1,0:T(8,128)(2,1)S(1)} %collective-permute-done.2) | copy-start | bytes 540676
  60.7 7.5 %collective-permute-start.3 = (bf16[704,128]{1,0:T(8,128)(2,1)S(1)}, bf16[704,128]{1,0:T(8,128)(2,1)S(1)}, u32[]{:S(2)}, u32[]{:S(2)}) collective-permute-start(bf16[704,128]{1,0:T(8,128)(2,1)S(1)} %collective-permute-done.2), channel_id=1, source_target_pairs={{0,8},{8,16},{16,24},{24,32},{32,40},{40,48},{48,56},{56,64},{64,7... | collective-permute-start | bytes 540680 | tf_op jit(solution)/shard_map/ppermute | solution.py:27
  61.7 6.6 %collective-permute-start.11 = (bf16[704,128]{1,0:T(8,128)(2,1)S(1)}, bf16[704,128]{1,0:T(8,128)(2,1)S(1)}, u32[]{:S(2)}, u32[]{:S(2)}) collective-permute-start(bf16[704,128]{1,0:T(8,128)(2,1)S(1)} %collective-permute-done.10), channel_id=1, source_target_pairs={{8,0},{16,8},{24,16},{32,24},{40,32},{48,40},{56,48},{64,56},{72,6... | collective-permute-start | bytes 540680 | tf_op jit(solution)/shard_map/ppermute | solution.py:29
  68.2 7.2 %copy-start.24 = (bf16[704,128]{1,0:T(8,128)(2,1)}, bf16[704,128]{1,0:T(8,128)(2,1)S(1)}, u32[]{:S(2)}) copy-start(bf16[704,128]{1,0:T(8,128)(2,1)S(1)} %collective-permute-done.3) | copy-start | bytes 540676
  68.2 7.2 %collective-permute-start.4 = (bf16[704,128]{1,0:T(8,128)(2,1)S(1)}, bf16[704,128]{1,0:T(8,128)(2,1)S(1)}, u32[]{:S(2)}, u32[]{:S(2)}) collective-permute-start(bf16[704,128]{1,0:T(8,128)(2,1)S(1)} %collective-permute-done.3), channel_id=1, source_target_pairs={{0,8},{8,16},{16,24},{24,32},{32,40},{40,48},{48,56},{56,64},{64,7... | collective-permute-start | bytes 540680 | tf_op jit(solution)/shard_map/ppermute | solution.py:27
  68.3 22.5 %copy-start.19 = (bf16[704,128]{1,0:T(8,128)(2,1)}, bf16[704,128]{1,0:T(8,128)(2,1)S(1)}, u32[]{:S(2)}) copy-start(bf16[704,128]{1,0:T(8,128)(2,1)S(1)} %collective-permute-done.11) | copy-start | bytes 540676
  68.3 9.0 %collective-permute-start.12 = (bf16[704,128]{1,0:T(8,128)(2,1)S(1)}, bf16[704,128]{1,0:T(8,128)(2,1)S(1)}, u32[]{:S(2)}, u32[]{:S(2)}) collective-permute-start(bf16[704,128]{1,0:T(8,128)(2,1)S(1)} %collective-permute-done.11), channel_id=1, source_target_pairs={{8,0},{16,8},{24,16},{32,24},{40,32},{48,40},{56,48},{64,56},{72,6... | collective-permute-start | bytes 540680 | tf_op jit(solution)/shard_map/ppermute | solution.py:29
  75.4 15.3 %copy-start.26 = (bf16[704,128]{1,0:T(8,128)(2,1)}, bf16[704,128]{1,0:T(8,128)(2,1)S(1)}, u32[]{:S(2)}) copy-start(bf16[704,128]{1,0:T(8,128)(2,1)S(1)} %collective-permute-done.4) | copy-start | bytes 540676
  75.4 7.2 %collective-permute-start.5 = (bf16[704,128]{1,0:T(8,128)(2,1)S(1)}, bf16[704,128]{1,0:T(8,128)(2,1)S(1)}, u32[]{:S(2)}, u32[]{:S(2)}) collective-permute-start(bf16[704,128]{1,0:T(8,128)(2,1)S(1)} %collective-permute-done.4), channel_id=1, source_target_pairs={{0,8},{8,16},{16,24},{24,32},{32,40},{40,48},{48,56},{56,64},{64,7... | collective-permute-start | bytes 540680 | tf_op jit(solution)/shard_map/ppermute | solution.py:27
  76.2 23.8 %copy-start.31 = (f32[2048]{0:T(1024)S(1)}, f32[2048]{0:T(1024)}, u32[]{:S(2)}) copy-start(f32[2048]{0:T(1024)} %param.18) | copy-start | bytes 24580
  77.3 13.4 %copy-start.21 = (bf16[704,128]{1,0:T(8,128)(2,1)}, bf16[704,128]{1,0:T(8,128)(2,1)S(1)}, u32[]{:S(2)}) copy-start(bf16[704,128]{1,0:T(8,128)(2,1)S(1)} %collective-permute-done.12) | copy-start | bytes 540676
  77.3 7.2 %collective-permute-start.13 = (bf16[704,128]{1,0:T(8,128)(2,1)S(1)}, bf16[704,128]{1,0:T(8,128)(2,1)}, u32[]{:S(2)}, u32[]{:S(2)}) collective-permute-start(bf16[704,128]{1,0:T(8,128)(2,1)S(1)} %collective-permute-done.12), channel_id=1, source_target_pairs={{8,0},{16,8},{24,16},{32,24},{40,32},{48,40},{56,48},{64,56},{72,6... | collective-permute-start | bytes 540680 | tf_op jit(solution)/shard_map/ppermute | solution.py:29
  82.6 8.1 %copy-start.28 = (bf16[704,128]{1,0:T(8,128)(2,1)}, bf16[704,128]{1,0:T(8,128)(2,1)S(1)}, u32[]{:S(2)}) copy-start(bf16[704,128]{1,0:T(8,128)(2,1)S(1)} %collective-permute-done.5) | copy-start | bytes 540676
  82.6 7.0 %collective-permute-start.6 = (bf16[704,128]{1,0:T(8,128)(2,1)S(1)}, bf16[704,128]{1,0:T(8,128)(2,1)}, u32[]{:S(2)}, u32[]{:S(2)}) collective-permute-start(bf16[704,128]{1,0:T(8,128)(2,1)S(1)} %collective-permute-done.5), channel_id=1, source_target_pairs={{0,8},{8,16},{16,24},{24,32},{32,40},{40,48},{48,56},{56,64},{64,7... | collective-permute-start | bytes 540680 | tf_op jit(solution)/shard_map/ppermute | solution.py:27
  84.6 121.6 %collective-permute-start.14 = (bf16[704,128]{1,0:T(8,128)(2,1)}, bf16[704,128]{1,0:T(8,128)(2,1)}, u32[]{:S(2)}, u32[]{:S(2)}) collective-permute-start(bf16[704,128]{1,0:T(8,128)(2,1)} %collective-permute-done.13), channel_id=1, source_target_pairs={{8,0},{16,8},{24,16},{32,24},{40,32},{48,40},{56,48},{64,56},{72,6... | collective-permute-start | bytes 540680 | tf_op jit(solution)/shard_map/ppermute | solution.py:29
  89.6 77.0 %collective-permute-start.7 = (bf16[704,128]{1,0:T(8,128)(2,1)}, bf16[704,128]{1,0:T(8,128)(2,1)}, u32[]{:S(2)}, u32[]{:S(2)}) collective-permute-start(bf16[704,128]{1,0:T(8,128)(2,1)} %collective-permute-done.6), channel_id=1, source_target_pairs={{0,8},{8,16},{16,24},{24,32},{32,40},{40,48},{48,56},{56,64},{64,7... | collective-permute-start | bytes 540680 | tf_op jit(solution)/shard_map/ppermute | solution.py:27
  90.7 53.9 %all-to-all-start.1 = ((bf16[16,256,128]{1,2,0:T(8,128)(2,1)}), bf16[16,256,128]{1,2,0:T(8,128)(2,1)S(1)}, u32[]{:S(2)}, u32[]{:S(2)}) async-start(bf16[16,256,128]{1,2,0:T(8,128)(2,1)} %broadcast_in_dim.49), calls=%async_computation.1 | async-start | bytes 2097152 | tf_op jit(solution)/shard_map/all_to_all | solution.py:38
  112.1 7.3 %copy-start.3 = (f32[8,64,128]{2,0,1:T(8,128)S(1)}, f32[8,64,128]{2,0,1:T(8,128)}, u32[]{:S(2)}) copy-start(f32[8,64,128]{2,0,1:T(8,128)} %copy-done.2) | copy-start | bytes 786436
  113.2 31.5 %copy-start.35 = (f32[256]{0:T(256)S(1)}, f32[256]{0:T(256)}, u32[]{:S(2)}) copy-start(f32[256]{0:T(256)} %param.25) | copy-start | bytes 3076
  146.9 24.6 %copy-start.27 = (bf16[704,128]{1,0:T(8,128)(2,1)S(1)}, bf16[704,128]{1,0:T(8,128)(2,1)}, u32[]{:S(2)}) copy-start(bf16[704,128]{1,0:T(8,128)(2,1)} %copy-done.26) | copy-start | bytes 540676
  146.9 25.3 %copy-start.25 = (bf16[704,128]{1,0:T(8,128)(2,1)S(1)}, bf16[704,128]{1,0:T(8,128)(2,1)}, u32[]{:S(2)}) copy-start(bf16[704,128]{1,0:T(8,128)(2,1)} %copy-done.24) | copy-start | bytes 540676
  146.9 26.0 %copy-start.23 = (bf16[704,128]{1,0:T(8,128)(2,1)S(1)}, bf16[704,128]{1,0:T(8,128)(2,1)}, u32[]{:S(2)}) copy-start(bf16[704,128]{1,0:T(8,128)(2,1)} %copy-done.22) | copy-start | bytes 540676
  146.9 26.7 %copy-start.18 = (bf16[704,128]{1,0:T(8,128)(2,1)S(1)}, bf16[704,128]{1,0:T(8,128)(2,1)}, u32[]{:S(2)}) copy-start(bf16[704,128]{1,0:T(8,128)(2,1)} %copy-done.17) | copy-start | bytes 540676
  146.9 27.4 %copy-start.14 = (bf16[704,128]{1,0:T(8,128)(2,1)S(1)}, bf16[704,128]{1,0:T(8,128)(2,1)}, u32[]{:S(2)}) copy-start(bf16[704,128]{1,0:T(8,128)(2,1)} %copy-done.13) | copy-start | bytes 540676
  146.9 45.9 %all-to-all-start.2 = ((bf16[8,512,256]{2,1,0:T(8,128)(2,1)}), bf16[8,512,256]{2,1,0:T(8,128)(2,1)S(1)}, u32[]{:S(2)}, u32[]{:S(2)}) async-start(bf16[8,512,256]{2,1,0:T(8,128)(2,1)} %bitcast.136), calls=%async_computation.2 | async-start | bytes 4194304 | tf_op jit(solution)/shard_map/all_to_all | solution.py:68
  166.6 26.5 %copy-start.6 = (bf16[512,256]{1,0:T(8,128)(2,1)S(1)}, bf16[512,256]{1,0:T(8,128)(2,1)}, u32[]{:S(2)}) copy-start(bf16[512,256]{1,0:T(8,128)(2,1)} %param.17) | copy-start | bytes 786436
  193.3 6.2 %copy-start.8 = (bf16[704,128]{1,0:T(8,128)(2,1)S(1)}, bf16[704,128]{1,0:T(8,128)(2,1)}, u32[]{:S(2)}) copy-start(bf16[704,128]{1,0:T(8,128)(2,1)} %param.30) | copy-start | bytes 540676
  193.3 6.9 %copy-start.10 = (bf16[704,128]{1,0:T(8,128)(2,1)S(1)}, bf16[704,128]{1,0:T(8,128)(2,1)}, u32[]{:S(2)}) copy-start(bf16[704,128]{1,0:T(8,128)(2,1)} %copy-done.9) | copy-start | bytes 540676
  194.9 6.7 %copy-start.16 = (bf16[704,128]{1,0:T(8,128)(2,1)S(1)}, bf16[704,128]{1,0:T(8,128)(2,1)}, u32[]{:S(2)}) copy-start(bf16[704,128]{1,0:T(8,128)(2,1)} %copy-done.15) | copy-start | bytes 540676
  194.9 7.4 %copy-start.20 = (bf16[704,128]{1,0:T(8,128)(2,1)S(1)}, bf16[704,128]{1,0:T(8,128)(2,1)}, u32[]{:S(2)}) copy-start(bf16[704,128]{1,0:T(8,128)(2,1)} %copy-done.19) | copy-start | bytes 540676
  194.9 30.9 %all-to-all-start.3 = ((bf16[8,512,256]{1,2,0:T(8,128)(2,1)}), bf16[8,512,256]{1,2,0:T(8,128)(2,1)S(1)}, u32[]{:S(2)}, u32[]{:S(2)}) async-start(bf16[8,512,256]{1,2,0:T(8,128)(2,1)} %broadcast_in_dim.50), calls=%async_computation.3 | async-start | bytes 4194304 | tf_op jit(solution)/shard_map/all_to_all | solution.py:38
  207.8 18.6 %copy-start.33 = (f32[2048]{0:T(1024)S(1)}, f32[2048]{0:T(1024)}, u32[]{:S(2)}) copy-start(f32[2048]{0:T(1024)} %param.27) | copy-start | bytes 24580
  240.7 45.0 %copy-start.34 = (f32[256]{0:T(256)S(1)}, f32[256]{0:T(256)}, u32[]{:S(2)}) copy-start(f32[256]{0:T(256)} %param.31) | copy-start | bytes 3076
  (11 other events, 26.5 us)
Sparse Core Ops, SparseCore 0:
  9.1 80.0 all-gather.2
  91.0 132.4 all-gather.4
